TPU v7x, 32 devices: a whole 2x2x4 slice. The times are simulated.
32 devices in a mesh: grp: 2 (over y), ep: 4 (over z), tp: 4 (over x, core).
Axes of the slice: x: 2, y: 2, z: 4, core: 2. Of those that a mesh axis runs over, the one named last changes fastest.
Arguments:
- query_rows: bfloat16 [1536, 2048], P(('grp', 'ep'), 'tp'), parts along dimension 0, may hold values from -100 to 100
- projected_keys: bfloat16 [1536, 512], P(('grp', 'ep'), 'tp'), parts along dimension 0, may hold values from -100 to 100
- projected_values: bfloat16 [1536, 512], P(('grp', 'ep'), 'tp'), parts along dimension 0, may hold values from -6 to 6
- query_gain: float32 [128], replicated, may hold values from 0.3 to 6.5
- key_norm_gain: float32 [128], replicated, may hold values from 0.3 to 6.5
- out_proj: bfloat16 [2048, 2048], P('tp'), may hold values from -4 to 4
- mix_tokens: bfloat16 [4096, 2048], P(('grp', 'ep', 'tp')), parts along dimension 0, may hold values from -150 to 150
- norm_gain: float32 [2048], replicated, may hold values from 0.1 to 1.9
- expert_ids: int32 [4096, 2], P(('grp', 'ep', 'tp')), parts along dimension 0, may hold values from 0 to 3, all different within a row; in each aligned block of 128 rows (0 to 127, 128 to 255, ...) at most 96 rows name the same one
- expert_score: float32 [4096, 2], P(('grp', 'ep', 'tp')), parts along dimension 0, may hold values from -6 to 6
- gate_proj: bfloat16 [4, 2048, 2048], P('ep', None, 'tp'), may hold values from -0.125 to 0.125
- up_proj: bfloat16 [4, 2048, 2048], P('ep', None, 'tp'), may hold values from -0.125 to 0.125
- down_proj: bfloat16 [4, 2048, 2048], P('ep', 'tp'), may hold values from -0.125 to 0.125
Outputs:
- mixed_rows: bfloat16 [1536, 2048], P(('grp', 'ep', 'tp')), parts along dimension 0
- expert_out: bfloat16 [4096, 2048], P(('grp', 'ep', 'tp')), parts along dimension 0
There are 2 independent parts, one for each index of `grp`. A program takes and returns all parts, laid end to end along the dimension named above; an argument that names none is the same for every part. Nothing has to cross between parts.
Inputs may be any that keep to these rules, and one draw needn't show every extreme that they name: `expert_ids`: each row names 2 different experts. Within the rows of one device (aligned blocks of 128 rows) no expert is named more than 96 times, and in every draw some device names some expert exactly 96 times.
All inputs are finite; a program needn't handle non-finite values.
Results may differ from a plain program's by a relative error of at most 0.014.
The roundings to bfloat16 on the way count: a program that leaves them out, or rounds other values in their place, can miss the bound.
Values may be sent and summed in bfloat16 or wider, within the bound.
A program may use at most 128 MiB of HBM per device.

v0:
```python
import math

import jax
import jax.numpy as jnp
from jax import lax
from jax.sharding import PartitionSpec as P

GRID_W = 64


EPS = 1e-06
THETA = 10000.0


def head_norm(vectors, gain):
    return vectors * lax.rsqrt(jnp.mean(vectors * vectors, axis=-1, keepdims=True) + EPS) * gain


def rotate_grid(vectors, token_positions):
    length, heads, head_dim = vectors.shape
    quarter = head_dim // 4
    freqs = 1.0 / THETA ** (jnp.arange(quarter, dtype=jnp.float32) * 4.0 / head_dim)
    grid_row = (token_positions // GRID_W).astype(jnp.float32)
    grid_col = (token_positions % GRID_W).astype(jnp.float32)
    angles = jnp.stack([grid_row[:, None] * freqs, grid_col[:, None] * freqs], axis=1)
    cosine = jnp.cos(angles)[:, None]
    sine = jnp.sin(angles)[:, None]
    halves = vectors.reshape(length, heads, 2, 2, quarter)
    first = halves[..., 0, :]
    second = halves[..., 1, :]
    turned = jnp.stack([first * cosine - second * sine, second * cosine + first * sine], axis=-2)
    return turned.reshape(length, heads, head_dim)


def prepare_inputs(raw_rows, gain, heads, token_positions):
    length = raw_rows.shape[0]
    head_dim = gain.shape[0]
    vectors = raw_rows.astype(jnp.float32).reshape(length, heads, head_dim)
    return rotate_grid(head_norm(vectors, gain), token_positions).astype(jnp.bfloat16)


def mixer_half(query_rows, projected_keys, projected_values, query_gain, key_norm_gain, out_proj):
    length = query_rows.shape[0]
    head_dim = query_gain.shape[0]
    kv_heads = projected_keys.shape[1] // head_dim
    q_heads = query_rows.shape[1] // head_dim
    queries_per_group = q_heads // kv_heads
    token_positions = lax.axis_index("ep") * length + jnp.arange(length, dtype=jnp.int32)
    query_matrix = prepare_inputs(query_rows, query_gain, q_heads, token_positions).reshape(
        length, kv_heads, queries_per_group, head_dim
    )
    keys_turned = prepare_inputs(projected_keys, key_norm_gain, kv_heads, token_positions).reshape(
        length, kv_heads * head_dim
    )
    score_scale = head_dim ** (-0.5)
    initial = (
        jnp.full((kv_heads, queries_per_group, length), -1e30, jnp.float32),
        jnp.zeros((kv_heads, queries_per_group, length), jnp.float32),
        jnp.zeros((length, kv_heads, queries_per_group, head_dim), jnp.float32),
    )
    key_piece = lax.all_gather(keys_turned, "ep", axis=0, tiled=True)
    value_piece = lax.all_gather(projected_values, "ep", axis=0, tiled=True)
    piece_rows = key_piece.shape[0]
    step_rows = math.gcd(piece_rows, 1024)

    def one_block(block_index, running):
        run_max, run_sum, run_acc = running
        offset = block_index * step_rows
        key_block = lax.dynamic_slice_in_dim(key_piece, offset, step_rows, 0).reshape(
            step_rows, kv_heads, head_dim
        )
        value_block = lax.dynamic_slice_in_dim(value_piece, offset, step_rows, 0).reshape(
            step_rows, kv_heads, head_dim
        )
        scores = (
            jnp.einsum(
                "tkgd,skd->kgts", query_matrix, key_block, preferred_element_type=jnp.float32
            )
            * score_scale
        )
        new_max = jnp.maximum(run_max, jnp.max(scores, axis=-1))
        factor = jnp.exp(run_max - new_max)
        weights = jnp.exp(scores - new_max[..., None])
        run_sum = run_sum * factor + jnp.sum(weights, axis=-1)
        update = jnp.einsum(
            "kgts,skd->tkgd",
            weights.astype(jnp.bfloat16),
            value_block,
            preferred_element_type=jnp.float32,
        )
        run_acc = run_acc * jnp.transpose(factor, (2, 0, 1))[..., None] + update
        return (new_max, run_sum, run_acc)

    run_max, run_sum, run_acc = lax.fori_loop(0, piece_rows // step_rows, one_block, initial)
    heads_out = (
        (run_acc / jnp.transpose(run_sum, (2, 0, 1))[..., None])
        .astype(jnp.bfloat16)
        .reshape(length, q_heads * head_dim)
    )
    return lax.psum_scatter(
        jnp.dot(heads_out, out_proj, preferred_element_type=jnp.float32).astype(jnp.bfloat16),
        "tp",
        scatter_dimension=0,
        tiled=True,
    )


def expert_half(mix_tokens, norm_gain, expert_ids, expert_score, gate_proj, up_proj, down_proj):
    length, model_dim = mix_tokens.shape
    top_count = expert_ids.shape[1]
    local_experts = gate_proj.shape[0]
    expert_axis = lax.axis_size("ep")
    experts_all = expert_axis * local_experts
    capacity = length * top_count * 3 // (2 * experts_all)
    values_b = mix_tokens.astype(jnp.float32)
    normed = (
        values_b
        * lax.rsqrt(jnp.mean(values_b * values_b, axis=-1, keepdims=True) + EPS)
        * norm_gain
    ).astype(jnp.bfloat16)
    flat = expert_ids.reshape(length * top_count)
    onehot = (flat[:, None] == jnp.arange(experts_all, dtype=jnp.int32)).astype(jnp.int32)
    slots = jnp.sum((jnp.cumsum(onehot, axis=0) - onehot) * onehot, axis=1)
    target = flat * capacity + slots
    placed = (target[:, None] == jnp.arange(experts_all * capacity, dtype=jnp.int32)).astype(
        jnp.int32
    )
    placed = jnp.sum(placed.reshape(length, top_count, experts_all * capacity), axis=1).astype(
        jnp.bfloat16
    )
    outgoing = jnp.einsum("re,rd->ed", placed, normed, preferred_element_type=jnp.float32).astype(
        jnp.bfloat16
    )
    outgoing = outgoing.reshape(expert_axis, local_experts, capacity, model_dim)
    rows_in = lax.all_gather(
        lax.all_to_all(outgoing, "ep", split_axis=0, concat_axis=0, tiled=True),
        "tp",
        axis=0,
        tiled=True,
    )
    gate_out = jnp.einsum("secd,edf->secf", rows_in, gate_proj, preferred_element_type=jnp.float32)
    up_out = jnp.einsum("secd,edf->secf", rows_in, up_proj, preferred_element_type=jnp.float32)
    active = (jax.nn.silu(gate_out) * up_out).astype(jnp.bfloat16)
    summed = lax.psum_scatter(
        jnp.einsum("secf,efd->secd", active, down_proj, preferred_element_type=jnp.float32).astype(
            jnp.bfloat16
        ),
        "tp",
        scatter_dimension=0,
        tiled=True,
    )
    returned = lax.all_to_all(summed, "ep", split_axis=0, concat_axis=0, tiled=True)
    results = returned.reshape(experts_all * capacity, model_dim)
    selected_expert = target.reshape(length, top_count)
    first_weight = jax.nn.sigmoid(expert_score[:, 0] - expert_score[:, 1])
    combined = first_weight[:, None] * results[selected_expert[:, 0]].astype(jnp.float32) + (
        1.0 - first_weight
    )[:, None] * results[selected_expert[:, 1]].astype(jnp.float32)
    return combined.astype(jnp.bfloat16)


def local(
    query_rows,
    projected_keys,
    projected_values,
    query_gain,
    key_norm_gain,
    out_proj,
    mix_tokens,
    norm_gain,
    expert_ids,
    expert_score,
    gate_proj,
    up_proj,
    down_proj,
):
    mixed_rows = mixer_half(
        query_rows, projected_keys, projected_values, query_gain, key_norm_gain, out_proj
    )
    expert_out = expert_half(
        mix_tokens, norm_gain, expert_ids, expert_score, gate_proj, up_proj, down_proj
    )
    return (mixed_rows, expert_out)


def solution(mesh):
    in_specs = (
        P(("grp", "ep"), "tp"),
        P(("grp", "ep"), "tp"),
        P(("grp", "ep"), "tp"),
        P(),
        P(),
        P("tp", None),
        P(("grp", "ep", "tp"), None),
        P(),
        P(("grp", "ep", "tp"), None),
        P(("grp", "ep", "tp"), None),
        P("ep", None, "tp"),
        P("ep", None, "tp"),
        P("ep", "tp", None),
    )
    out_specs = (P(("grp", "ep", "tp"), None), P(("grp", "ep", "tp"), None))
    return jax.shard_map(local, mesh=mesh, in_specs=in_specs, out_specs=out_specs, check_vma=False)
```

profile of v0, /device:TPU:0, one launch (start us, length us, event | category | flops | bytes accessed | tf_op | source)
XLA Modules:
  0.0 237.6 jit_solution(8891725918785150637)
XLA Ops:
  7.2 0.9 copy.76
  8.4 1.2 reduce-window.6
  11.1 1.2 fusion.39
  12.3 1.7 convolution_convert_fusion
  14.1 43.2 %all_to_all.10 = bf16[4,1,96,2048]{3,2,1,0:T(8,128)(2,1)} all-to-all(bf16[4,1,96,2048]{3,2,1,0:T(8,128)(2,1)S(1)} %bitcast.175), channel_id=1, replica_groups=mesh['grp'=2,'ep'=4,'tp'=4] {'ep'}, dimensions={0} | all-to-all | bytes 3145728 | tf_op jit(solution)/shard_map/all_to_all | solution.py:136
  57.4 45.6 %all-gather.2.cloned.1.call-done = bf16[16,1,96,2048]{3,2,1,0:T(8,128)(2,1)} async-done(((bf16[4,1,96,2048]{3,2,1,0:T(8,128)(2,1)}), bf16[16,1,96,2048]{3,2,1,0:T(8,128)(2,1)}) %all-gather.2.cloned.1.call-update) | async-done | bytes 6291472 | tf_op jit(solution)/shard_map/all_gather | solution.py:135
  103.0 8.5 %fusion.15 = f32[16,96,512]{2,1,0:T(8,128)} fusion(bf16[16,1,96,2048]{3,2,1,0:T(8,128)(2,1)} %all-gather.2.cloned.1.call-done, bf16[1,2048,512]{2,1,0:T(8,128)(2,1)} %param.26), kind=kOutput, calls=%fused_computation.24 | convolution fusion | flops 3221225472 | bytes 11534336 | tf_op jit(solution)/shard_map/secd,edf->secf/dot_general | solution.py:142
  111.5 11.9 %convert_bitcast_fusion = bf16[16,1,96,2048]{3,2,0,1:T(8,128)(2,1)} fusion(bf16[1,512,2048]{2,1,0:T(8,128)(2,1)S(1)} %copy-done, f32[16,96,512]{2,1,0:T(8,128)} %fusion.15, bf16[1,2048,512]{2,1,0:T(8,128)(2,1)} %param.25, bf16[16,1,96,2048]{3,2,1,0:T(8,128)(2,1)} %all-gather.2.cloned.1.call-done), kind=kOutput, calls=%fused_computation.28 | convolution fusion | flops 6450315264 | bytes 19922944 | tf_op jit(solution)/shard_map/secf,efd->secd/dot_general | solution.py:145
  126.1 14.4 %all_gather.9 = bf16[768,128]{1,0:T(8,128)(2,1)} all-gather(bf16[192,128]{1,0:T(8,128)(2,1)S(1)} %copy.72), channel_id=1, replica_groups=mesh['grp'=2,'ep'=4,'tp'=4] {'ep'}, dimensions={0}, use_global_device_ids=true | all-gather | bytes 245760 | tf_op jit(solution)/shard_map/all_gather | solution.py:61
  140.5 14.8 %all_gather.10 = bf16[768,128]{1,0:T(8,128)(2,1)} all-gather(bf16[192,128]{1,0:T(8,128)(2,1)S(1)} %copy-done.3), channel_id=1, replica_groups=mesh['grp'=2,'ep'=4,'tp'=4] {'ep'}, dimensions={0}, use_global_device_ids=true | all-gather | bytes 245760 | tf_op jit(solution)/shard_map/all_gather | solution.py:62
  155.2 27.2 %reduce-scatter.5.cloned.1.call-done = bf16[4,1,96,2048]{3,2,0,1:T(8,128)(2,1)} async-done(((bf16[16,1,96,2048]{3,2,0,1:T(8,128)(2,1)}), bf16[4,1,96,2048]{3,2,0,1:T(8,128)(2,1)}) %reduce-scatter.5.cloned.1.call-update) | async-done | bytes 1572880 | tf_op jit(solution)/shard_map/reduce_scatter | solution.py:144
  182.4 4.6 %all-to-all-start.1 = ((bf16[4,1,96,2048]{3,2,1,0:T(8,128)(2,1)}), bf16[4,1,96,2048]{3,2,1,0:T(8,128)(2,1)}, u32[]{:S(2)}, u32[]{:S(2)}) async-start(bf16[4,1,96,2048]{3,2,1,0:T(8,128)(2,1)} %bitcast.179), calls=%async_computation.3 | async-start | bytes 3145728 | tf_op jit(solution)/shard_map/all_to_all | solution.py:152
  187.0 8.8 %while.18 = (s32[]{:T(128)}, f32[1,4,192]{2,1,0:T(4,128)S(1)}, f32[1,4,192]{2,1,0:T(4,128)S(1)}, f32[192,1,4,128]{3,0,2,1:T(8,128)S(1)}, bf16[768,128]{1,0:T(8,1...) while((s32[]{:T(128)}, f32[1,4,192]{2,1,0:T(4,128)S(1)}, ...), condition=%wide.region_5.6_spmd.clone, body=%wide.region_2.5_spmd.clone.sunk | while | flops 102142472 | bytes 3522735 | solution.py:94
  187.0 1.2 fusion.75
  188.3 1.2 fusion.78
  189.9 1.3 fusion.75
  191.2 1.2 fusion.78
  192.9 1.3 fusion.75
  194.2 1.2 fusion.78
  196.2 3.1 %convolution_convert_fusion.1 = bf16[192,2048]{1,0:T(8,128)(2,1)} fusion(bf16[512,2048]{1,0:T(8,128)(2,1)} %param.20, bf16[24,8,4,128]{3,2,1,0:T(4,128)(2,1)S(1)} %bitcast.181), kind=kOutput, calls=%fused_computation.37 | convolution fusion | flops 403046400 | bytes 3080192 | tf_op jit(solution)/shard_map/dot_general | solution.py:101
  199.3 24.6 %all-to-all-done.1 = bf16[4,1,96,2048]{3,2,1,0:T(8,128)(2,1)} async-done(((bf16[4,1,96,2048]{3,2,1,0:T(8,128)(2,1)}), bf16[4,1,96,2048]{3,2,1,0:T(8,128)(2,1)}, u32[]{:S(2)}, u32[]{:S(2)}) %all-to-all-start.1) | async-done | bytes 1572896 | tf_op jit(solution)/shard_map/all_to_all | solution.py:152
  223.9 3.0 %gather_fusion = bf16[128,2048]{1,0:T(8,128)(2,1)S(1)} fusion(bf16[384,2048]{1,0:T(8,128)(2,1)} %bitcast.34, s32[1024]{0:T(1024)S(1)} %get-tuple-element.225), kind=kCustom, calls=%fused_computation | custom fusion | bytes 1049088 | tf_op jit(solution)/shard_map/gather | solution.py:156
  227.0 3.1 %gather_fusion.1 = bf16[128,2048]{1,0:T(8,128)(2,1)S(1)} fusion(bf16[384,2048]{1,0:T(8,128)(2,1)} %bitcast.34, s32[1024]{0:T(1024)S(1)} %get-tuple-element.224), kind=kCustom, calls=%fused_computation.1 | custom fusion | bytes 1049088 | tf_op jit(solution)/shard_map/gather | solution.py:158
  230.0 1.0 add_convert_fusion
  (75 shorter events, 5.9 us)
Async XLA Ops:
  7.2 104.3 %copy-start = (bf16[1,512,2048]{2,1,0:T(8,128)(2,1)S(1)}, bf16[1,512,2048]{2,1,0:T(8,128)(2,1)}, u32[]{:S(2)}) copy-start(bf16[1,512,2048]{2,1,0:T(8,128)(2,1)} %param.27) | copy-start | bytes 6291460
  7.2 95.8 %all-gather.2.cloned.1.call-start = ((), (), s32[]{:S(2)}) async-start(), calls=%async_computation.5 | async-start | bytes 7864320 | tf_op jit(solution)/shard_map/all_gather | solution.py:135
  57.3 125.1 %reduce-scatter.5.cloned.1.call-start = ((), (), s32[]{:S(2)}) async-start(), calls=%async_computation.6 | async-start | bytes 7864320 | tf_op jit(solution)/shard_map/reduce_scatter | solution.py:144
  123.4 0.9 copy-start.1
  123.4 1.1 copy-start.6
  123.4 2.0 copy-start.2
  123.4 2.2 copy-start.5
  124.9 15.6 %copy-start.3 = (bf16[192,128]{1,0:T(8,128)(2,1)S(1)}, bf16[192,128]{1,0:T(8,128)(2,1)}, u32[]{:S(2)}) copy-start(bf16[192,128]{1,0:T(8,128)(2,1)} %param.17) | copy-start | bytes 147460
  182.4 41.5 %all-to-all-start.1 = ((bf16[4,1,96,2048]{3,2,1,0:T(8,128)(2,1)}), bf16[4,1,96,2048]{3,2,1,0:T(8,128)(2,1)}, u32[]{:S(2)}, u32[]{:S(2)}) async-start(bf16[4,1,96,2048]{3,2,1,0:T(8,128)(2,1)} %bitcast.179), calls=%async_computation.3 | async-start | bytes 3145728 | tf_op jit(solution)/shard_map/all_to_all | solution.py:152
  187.0 44.1 %reduce-scatter.3.cloned.1.call-start = ((), (), s32[]{:S(2)}) async-start(), calls=%async_computation.4 | async-start | bytes 983040 | tf_op jit(solution)/shard_map/reduce_scatter | solution.py:100
  196.0 3.3 %copy-start.4 = (f32[128,2]{0,1:T(2,128)S(1)}, f32[128,2]{0,1:T(2,128)}, u32[]{:S(2)}) copy-start(f32[128,2]{0,1:T(2,128)} %param.24) | copy-start | bytes 3076
Sparse Core Ops, SparseCore 0:
  57.4 45.4 all-gather.1
  123.5 58.8 reduce-scatter.4
  199.4 23.6 reduce-scatter.2
where the time goes:
time: 238 us
  waiting for transfers between devices  97.5 us (41%)
  blocking collectives  72.3 us (30%)
  matrix products  32.6 us (14%)
  between operations  14 us (6%)
  local copies, waits for them, and re-layouts  9.41 us (4%)
  other arithmetic  6.92 us (3%)
  starting transfers between devices  4.68 us (2%)
    all_gather x1, waiting for transfers between devices, expert_half(): lax.all_gather(lax.all_to_all(outgoing, 'ep', split_axis=0, concat_axis=0...  45.6 us
    all_to_all x1, blocking collectives, expert_half(): lax.all_to_all(outgoing, 'ep', split_axis=0, concat_axis=0, tiled=True)  43.2 us
    reduce_scatter x1, waiting for transfers between devices, expert_half(): lax.psum_scatter(jnp.einsum('secf,efd->secd', active, down_proj, preferre...  27.2 us
    all_to_all x1, waiting for transfers between devices, expert_half(): lax.all_to_all(summed, 'ep', split_axis=0, concat_axis=0, tiled=True)  24.6 us
    all_gather x1, blocking collectives, mixer_half(): value_piece = lax.all_gather(projected_values, 'ep', axis=0, tiled=True)  14.8 us
    all_gather x1, blocking collectives, mixer_half(): key_piece = lax.all_gather(keys_turned, 'ep', axis=0, tiled=True)  14.4 us
    dot_general x1, matrix products, expert_half(): jnp.einsum('secf,efd->secd', active, down_proj, preferred_element_type=jn...  11.9 us
    dot_general x1, matrix products, expert_half(): jnp.einsum('secd,edf->secf', rows_in, up_proj, preferred_element_type=jnp...  8.52 us
  transfers between devices with their start and end apart: 4, of which 3 were waited for; matrix products, arithmetic and copies ran while one was open for 9% of the time, Pallas kernels for 0%

commit v1 on v0

--- a/solution.py
+++ b/solution.py
@@ -58,8 +58,12 @@
         jnp.zeros((kv_heads, queries_per_group, length), jnp.float32),
         jnp.zeros((length, kv_heads, queries_per_group, head_dim), jnp.float32),
     )
-    key_piece = lax.all_gather(keys_turned, "ep", axis=0, tiled=True)
-    value_piece = lax.all_gather(projected_values, "ep", axis=0, tiled=True)
+    width = kv_heads * head_dim
+    pair = lax.all_gather(
+        jnp.concatenate([keys_turned, projected_values], axis=1), "ep", axis=0, tiled=True
+    )
+    key_piece = pair[:, :width]
+    value_piece = pair[:, width:]
     piece_rows = key_piece.shape[0]
     step_rows = math.gcd(piece_rows, 1024)
 
@@ -97,15 +101,24 @@
         .astype(jnp.bfloat16)
         .reshape(length, q_heads * head_dim)
     )
-    return lax.psum_scatter(
-        jnp.dot(heads_out, out_proj, preferred_element_type=jnp.float32).astype(jnp.bfloat16),
-        "tp",
-        scatter_dimension=0,
-        tiled=True,
-    )
-
-
-def expert_half(mix_tokens, norm_gain, expert_ids, expert_score, gate_proj, up_proj, down_proj):
+    return jnp.dot(heads_out, out_proj, preferred_element_type=jnp.float32).astype(jnp.bfloat16)
+
+
+def both_halves(
+    query_rows,
+    projected_keys,
+    projected_values,
+    query_gain,
+    key_norm_gain,
+    out_proj,
+    mix_tokens,
+    norm_gain,
+    expert_ids,
+    expert_score,
+    gate_proj,
+    up_proj,
+    down_proj,
+):
     length, model_dim = mix_tokens.shape
     top_count = expert_ids.shape[1]
     local_experts = gate_proj.shape[0]
@@ -132,12 +145,16 @@
         jnp.bfloat16
     )
     outgoing = outgoing.reshape(expert_axis, local_experts, capacity, model_dim)
-    rows_in = lax.all_gather(
-        lax.all_to_all(outgoing, "ep", split_axis=0, concat_axis=0, tiled=True),
-        "tp",
-        axis=0,
-        tiled=True,
-    )
+    arrived = lax.all_to_all(outgoing, "ep", split_axis=0, concat_axis=0, tiled=True)
+    arrived, query_rows, projected_keys, projected_values = lax.optimization_barrier(
+        (arrived, query_rows, projected_keys, projected_values)
+    )
+    rows_in = lax.all_gather(arrived, "tp", axis=0, tiled=True)
+    head_partial = mixer_half(
+        query_rows, projected_keys, projected_values, query_gain, key_norm_gain, out_proj
+    )
+    rows_in, head_partial = lax.optimization_barrier((rows_in, head_partial))
+    mixed_rows = lax.psum_scatter(head_partial, "tp", scatter_dimension=0, tiled=True)
     gate_out = jnp.einsum("secd,edf->secf", rows_in, gate_proj, preferred_element_type=jnp.float32)
     up_out = jnp.einsum("secd,edf->secf", rows_in, up_proj, preferred_element_type=jnp.float32)
     active = (jax.nn.silu(gate_out) * up_out).astype(jnp.bfloat16)
@@ -151,12 +168,20 @@
     )
     returned = lax.all_to_all(summed, "ep", split_axis=0, concat_axis=0, tiled=True)
     results = returned.reshape(experts_all * capacity, model_dim)
-    selected_expert = target.reshape(length, top_count)
     first_weight = jax.nn.sigmoid(expert_score[:, 0] - expert_score[:, 1])
-    combined = first_weight[:, None] * results[selected_expert[:, 0]].astype(jnp.float32) + (
-        1.0 - first_weight
-    )[:, None] * results[selected_expert[:, 1]].astype(jnp.float32)
-    return combined.astype(jnp.bfloat16)
+    picks = target.reshape(length, top_count)
+    chosen = [
+        jnp.dot(
+            (picks[:, k : k + 1] == jnp.arange(experts_all * capacity, dtype=jnp.int32)).astype(
+                jnp.bfloat16
+            ),
+            results,
+            preferred_element_type=jnp.float32,
+        )
+        for k in range(2)
+    ]
+    combined = first_weight[:, None] * chosen[0] + (1.0 - first_weight)[:, None] * chosen[1]
+    return (mixed_rows, combined.astype(jnp.bfloat16))
 
 
 def local(
@@ -174,13 +199,21 @@
     up_proj,
     down_proj,
 ):
-    mixed_rows = mixer_half(
-        query_rows, projected_keys, projected_values, query_gain, key_norm_gain, out_proj
-    )
-    expert_out = expert_half(
-        mix_tokens, norm_gain, expert_ids, expert_score, gate_proj, up_proj, down_proj
-    )
-    return (mixed_rows, expert_out)
+    return both_halves(
+        query_rows,
+        projected_keys,
+        projected_values,
+        query_gain,
+        key_norm_gain,
+        out_proj,
+        mix_tokens,
+        norm_gain,
+        expert_ids,
+        expert_score,
+        gate_proj,
+        up_proj,
+        down_proj,
+    )
 
 
 def solution(mesh):

time: 238 us -> 236 us (level)
  blocking collectives: 72.3 us -> 58.4 us
  waiting for transfers between devices: 97.5 us -> 111 us
  local copies, waits for them, and re-layouts: 9.41 us -> 3.36 us
  matrix products: 32.6 us -> 37.2 us
    reduce_scatter x2, waiting for transfers between devices: 27.2 us -> 59 us  [the longest x1 59 us: both_halves(): lax.psum_scatter(jnp.einsum('secf,efd->secd', active, down_proj, preferre...]
    all_gather x1, waiting for transfers between devices: 45.6 us -> 15.6 us  [both_halves(): rows_in = lax.all_gather(arrived, 'tp', axis=0, tiled=True)]
    all_gather x2 -> x1, blocking collectives: 29.1 us -> 15.1 us  [mixer_half(): lax.all_gather(jnp.concatenate([keys_turned, projected_values], axis=1),...]
    all_to_all x1, waiting for transfers between devices: 24.6 us -> 36.1 us  [both_halves(): lax.all_to_all(summed, 'ep', split_axis=0, concat_axis=0, tiled=True)]
    gather x2 -> x0, local copies, waits for them, and re-layouts: 6.1 us -> none  [the longest x1 3.05 us: expert_half(): results[selected_expert[:, 1]].astype(jnp.float32)]
    dot_general x3 -> x5, matrix products: 22.1 us -> 26.7 us  [the longest x1 11.9 us: both_halves(): jnp.einsum('secf,efd->secd', active, down_proj, preferred_element_type=jn...]
  transfers between devices with their start and end apart: 4 -> 4, of which waited for: 3 -> 3; matrix products, arithmetic and copies ran while one was open for 9% -> 8% of each run, Pallas kernels for 0% -> 0%
where the time goes in v1:
time: 236 us; the launch traced here: 235 us
  waiting for transfers between devices  111 us (47%)
  blocking collectives  58.4 us (25%)
  matrix products  37.2 us (16%)
  between operations  14 us (6%)
  other arithmetic  5.9 us (2%)
  starting transfers between devices  4.68 us (2%)
  local copies, waits for them, and re-layouts  3.36 us (1%)
    reduce_scatter x1, waiting for transfers between devices, both_halves(): lax.psum_scatter(jnp.einsum('secf,efd->secd', active, down_proj, preferre...  59 us
    all_to_all x1, blocking collectives, both_halves(): lax.all_to_all(outgoing, 'ep', split_axis=0, concat_axis=0, tiled=True)  43.3 us
    all_to_all x1, waiting for transfers between devices, both_halves(): lax.all_to_all(summed, 'ep', split_axis=0, concat_axis=0, tiled=True)  36.1 us
    all_gather x1, waiting for transfers between devices, both_halves(): rows_in = lax.all_gather(arrived, 'tp', axis=0, tiled=True)  15.6 us
    all_gather x1, blocking collectives, mixer_half(): lax.all_gather(jnp.concatenate([keys_turned, projected_values], axis=1),...  15.1 us
    dot_general x1, matrix products, both_halves(): jnp.einsum('secf,efd->secd', active, down_proj, preferred_element_type=jn...  11.9 us
    dot_general x1, matrix products, both_halves(): jnp.einsum('secd,edf->secf', rows_in, up_proj, preferred_element_type=jnp...  8.52 us
  transfers between devices with their start and end apart: 4, of which 3 were waited for; matrix products, arithmetic and copies ran while one was open for 8% of the time, Pallas kernels for 0%

profile of v1, /device:TPU:0, one launch (start us, length us, event | category | flops | bytes accessed | tf_op | source)
XLA Modules:
  0.0 235.2 jit_solution(7432642397368163617)
XLA Ops:
  7.2 0.9 copy.77
  8.4 1.2 fusion.41
  9.7 1.2 reduce-window.6
  12.3 1.7 convolution_convert_fusion
  14.1 43.3 %all_to_all.10 = bf16[4,1,96,2048]{3,2,1,0:T(8,128)(2,1)} all-to-all(bf16[4,1,96,2048]{3,2,1,0:T(8,128)(2,1)S(1)} %bitcast.177), channel_id=1, replica_groups=mesh['grp'=2,'ep'=4,'tp'=4] {'ep'}, dimensions={0} | all-to-all | bytes 3145728 | tf_op jit(solution)/shard_map/all_to_all | solution.py:148
  59.5 15.1 %all_gather.7 = bf16[768,256]{1,0:T(8,128)(2,1)S(1)} all-gather(bf16[192,256]{1,0:T(8,128)(2,1)S(1)} %copy.85), channel_id=1, replica_groups=mesh['grp'=2,'ep'=4,'tp'=4] {'ep'}, dimensions={0}, use_global_device_ids=true | all-gather | bytes 491520 | tf_op jit(solution)/shard_map/all_gather | solution.py:62
  74.6 0.8 fusion.68
  75.3 8.8 %while.18 = (s32[]{:T(128)}, f32[1,4,192]{2,1,0:T(4,128)S(1)}, f32[1,4,192]{2,1,0:T(4,128)S(1)}, f32[192,1,4,128]{3,0,2,1:T(8,128)S(1)}, bf16[768,128]{1,0:T(8,1...) while((s32[]{:T(128)}, f32[1,4,192]{2,1,0:T(4,128)S(1)}, ...), condition=%wide.region_10.11_spmd.clone, body=%wide.region_7.10_spmd.clone.sunk | while | flops 102142472 | bytes 3522743 | solution.py:98
  75.3 1.2 fusion.80
  77.0 1.2 fusion.83
  78.3 1.2 fusion.80
  79.9 1.2 fusion.83
  81.2 1.3 fusion.80
  82.9 1.2 fusion.83
  84.4 3.1 %convolution_convert_fusion.1 = bf16[192,2048]{1,0:T(8,128)(2,1)} fusion(bf16[512,2048]{1,0:T(8,128)(2,1)} %param.20, bf16[24,8,4,128]{3,2,1,0:T(4,128)(2,1)S(1)} %bitcast.183), kind=kOutput, calls=%fused_computation.35 | convolution fusion | flops 403046400 | bytes 3080192 | tf_op jit(solution)/shard_map/dot_general | solution.py:104
  87.5 15.6 %all-gather.2.cloned.1.call-done = bf16[16,1,96,2048]{3,2,1,0:T(8,128)(2,1)} async-done(((bf16[4,1,96,2048]{3,2,1,0:T(8,128)(2,1)}), bf16[16,1,96,2048]{3,2,1,0:T(8,128)(2,1)}) %all-gather.2.cloned.1.call-update) | async-done | bytes 6291472 | tf_op jit(solution)/shard_map/all_gather | solution.py:152
  103.1 8.5 %fusion.15 = f32[16,96,512]{2,1,0:T(8,128)} fusion(bf16[16,1,96,2048]{3,2,1,0:T(8,128)(2,1)} %all-gather.2.cloned.1.call-done, bf16[1,2048,512]{2,1,0:T(8,128)(2,1)} %param.26), kind=kOutput, calls=%fused_computation.22 | convolution fusion | flops 3221225472 | bytes 11534336 | tf_op jit(solution)/shard_map/secd,edf->secf/dot_general | solution.py:159
  111.7 11.9 %convert_bitcast_fusion = bf16[16,1,96,2048]{3,2,0,1:T(8,128)(2,1)} fusion(bf16[1,512,2048]{2,1,0:T(8,128)(2,1)S(1)} %copy-done, f32[16,96,512]{2,1,0:T(8,128)} %fusion.15, bf16[1,2048,512]{2,1,0:T(8,128)(2,1)} %param.25, bf16[16,1,96,2048]{3,2,1,0:T(8,128)(2,1)} %all-gather.2.cloned.1.call-done), kind=kOutput, calls=%fused_computation.26 | convolution fusion | flops 6450315264 | bytes 19922944 | tf_op jit(solution)/shard_map/secf,efd->secd/dot_general | solution.py:162
  123.6 59.0 %reduce-scatter.5.cloned.1.call-done = bf16[4,1,96,2048]{3,2,0,1:T(8,128)(2,1)} async-done(((bf16[16,1,96,2048]{3,2,0,1:T(8,128)(2,1)}), bf16[4,1,96,2048]{3,2,0,1:T(8,128)(2,1)}) %reduce-scatter.5.cloned.1.call-update) | async-done | bytes 1572880 | tf_op jit(solution)/shard_map/reduce_scatter | solution.py:161
  182.6 4.6 %all-to-all-start.1 = ((bf16[4,1,96,2048]{3,2,1,0:T(8,128)(2,1)}), bf16[4,1,96,2048]{3,2,1,0:T(8,128)(2,1)}, u32[]{:S(2)}, u32[]{:S(2)}) async-start(bf16[4,1,96,2048]{3,2,1,0:T(8,128)(2,1)} %bitcast.181), calls=%async_computation.3 | async-start | bytes 3145728 | tf_op jit(solution)/shard_map/all_to_all | solution.py:169
  187.2 0.7 reduce-scatter.3.cloned.1.call-update
  187.9 36.1 %all-to-all-done.1 = bf16[4,1,96,2048]{3,2,1,0:T(8,128)(2,1)} async-done(((bf16[4,1,96,2048]{3,2,1,0:T(8,128)(2,1)}), bf16[4,1,96,2048]{3,2,1,0:T(8,128)(2,1)}, u32[]{:S(2)}, u32[]{:S(2)}) %all-to-all-start.1) | async-done | bytes 1572896 | tf_op jit(solution)/shard_map/all_to_all | solution.py:169
  224.1 1.9 convolution_multiply_fusion.2
  226.0 2.7 %fusion.24 = bf16[128,2048]{1,0:T(8,128)(2,1)} fusion(f32[128,2048]{1,0:T(8,128)S(1)} %convolution_multiply_fusion.2, bf16[384,2048]{1,0:T(8,128)(2,1)} %bitcast.35, f32[128]{0:T(128)S(1)} %get-tuple-element.216, s32[128]{0:T(128)S(1)} %get-tuple-element.232), kind=kOutput, calls=%fused_computation.39 | convolution fusion | flops 202162176 | bytes 3146752 | tf_op jit(solution)/shard_map/dot_general | solution.py:174
  (75 shorter events, 5.2 us)
Async XLA Ops:
  7.2 104.5 %copy-start = (bf16[1,512,2048]{2,1,0:T(8,128)(2,1)S(1)}, bf16[1,512,2048]{2,1,0:T(8,128)(2,1)}, u32[]{:S(2)}) copy-start(bf16[1,512,2048]{2,1,0:T(8,128)(2,1)} %param.27) | copy-start | bytes 6291460
  7.2 96.0 %all-gather.2.cloned.1.call-start = ((), (), s32[]{:S(2)}) async-start(), calls=%async_computation.4 | async-start | bytes 7864320 | tf_op jit(solution)/shard_map/all_gather | solution.py:152
  14.1 43.5 %copy-start.6 = (f32[128]{0:T(128)S(1)}, f32[128]{0:T(128)}, u32[]{:S(2)}) copy-start(f32[128]{0:T(128)} %param.18) | copy-start | bytes 1540
  14.1 43.9 %copy-start.2 = (bf16[192,128]{1,0:T(8,128)(2,1)S(1)}, bf16[192,128]{1,0:T(8,128)(2,1)}, u32[]{:S(2)}) copy-start(bf16[192,128]{1,0:T(8,128)(2,1)} %param.17) | copy-start | bytes 147460
  14.1 44.1 %copy-start.3 = (bf16[192,128]{1,0:T(8,128)(2,1)S(1)}, bf16[192,128]{1,0:T(8,128)(2,1)}, u32[]{:S(2)}) copy-start(bf16[192,128]{1,0:T(8,128)(2,1)} %param.16) | copy-start | bytes 147460
  14.1 44.2 %copy-start.5 = (f32[128]{0:T(128)S(1)}, f32[128]{0:T(128)}, u32[]{:S(2)}) copy-start(f32[128]{0:T(128)} %param.19) | copy-start | bytes 1540
  57.5 1.4 copy-start.1
  57.5 125.1 %reduce-scatter.5.cloned.1.call-start = ((), (), s32[]{:S(2)}) async-start(), calls=%async_computation.6 | async-start | bytes 7864320 | tf_op jit(solution)/shard_map/reduce_scatter | solution.py:161
  123.6 64.3 %copy-start.4 = (f32[128,2]{0,1:T(2,128)S(1)}, f32[128,2]{0,1:T(2,128)}, u32[]{:S(2)}) copy-start(f32[128,2]{0,1:T(2,128)} %param.24) | copy-start | bytes 3076
  182.6 41.5 %all-to-all-start.1 = ((bf16[4,1,96,2048]{3,2,1,0:T(8,128)(2,1)}), bf16[4,1,96,2048]{3,2,1,0:T(8,128)(2,1)}, u32[]{:S(2)}, u32[]{:S(2)}) async-start(bf16[4,1,96,2048]{3,2,1,0:T(8,128)(2,1)} %bitcast.181), calls=%async_computation.3 | async-start | bytes 3145728 | tf_op jit(solution)/shard_map/all_to_all | solution.py:169
  187.2 41.5 %reduce-scatter.3.cloned.1.call-start = ((), (), s32[]{:S(2)}) async-start(), calls=%async_computation.5 | async-start | bytes 983040 | tf_op jit(solution)/shard_map/reduce_scatter | solution.py:157
Sparse Core Ops, SparseCore 0:
  57.6 45.4 all-gather.1
  123.7 58.8 reduce-scatter.4
  191.1 23.7 reduce-scatter.2

commit v2 on v1

--- a/solution.py
+++ b/solution.py
@@ -1,13 +1,17 @@
+import functools
 import math
 
 import jax
 import jax.numpy as jnp
 from jax import lax
+from jax.experimental import pallas as pl
+from jax.experimental.pallas import tpu as pltpu
 from jax.sharding import PartitionSpec as P
 
 GRID_W = 64
 
 
+MESH = pl.DeviceIdType.MESH
 EPS = 1e-06
 THETA = 10000.0
 
@@ -102,6 +106,234 @@
         .reshape(length, q_heads * head_dim)
     )
     return jnp.dot(heads_out, out_proj, preferred_element_type=jnp.float32).astype(jnp.bfloat16)
+
+
+def flip(index, bits):
+    result, place = 0, 1
+    for _ in range(8):
+        mine = (index // place) % 2
+        result = result + place * ((1 - mine) if bits & place else mine)
+        place *= 2
+    return result
+
+
+def exchange_kernel(
+    steps,
+    out_ref,
+    gate_ref,
+    up_ref,
+    down_ref,
+    back_ref,
+    rows,
+    act,
+    part,
+    from_core,
+    to_x,
+    from_x,
+    total,
+    zs,
+    zr,
+    xs,
+    xr,
+    cs,
+    cr,
+    ps,
+    pr,
+    qs,
+    qr,
+    bs,
+    br,
+):
+    me = lax.axis_index("ep")
+    lane = lax.axis_index("tp")
+    peers = [flip(me, k) for k in range(steps)]
+    core, across = flip(lane, 1), flip(lane, 2)
+    cap, width = out_ref.shape[1], out_ref.shape[2]
+    hidden = gate_ref.shape[1]
+    tile = math.gcd(hidden, 256)
+    tile_out = math.gcd(width, 256)
+
+    barrier = pltpu.get_barrier_semaphore()
+    friends = [{"ep": peers[k], "tp": lane} for k in range(1, steps)]
+    friends += [{"ep": me, "tp": core}, {"ep": me, "tp": across}]
+    for friend in friends:
+        pl.semaphore_signal(barrier, inc=1, device_id=friend, device_id_type=MESH)
+    pl.semaphore_wait(barrier, len(friends))
+
+    def remote(src, dst, send, recv, ep_to, tp_to):
+        return pltpu.make_async_remote_copy(
+            src_ref=src,
+            dst_ref=dst,
+            send_sem=send,
+            recv_sem=recv,
+            device_id={"ep": ep_to, "tp": tp_to},
+            device_id_type=MESH,
+        )
+
+    z_in = [None] + [
+        remote(out_ref.at[peers[k]], rows.at[k, 0], zs.at[k], zr.at[k], peers[k], lane)
+        for k in range(1, steps)
+    ]
+    x_in = [
+        remote(
+            out_ref.at[me] if k == 0 else rows.at[k, 0],
+            rows.at[k, 1],
+            xs.at[k],
+            xr.at[k],
+            me,
+            across,
+        )
+        for k in range(steps)
+    ]
+    c_in = [
+        remote(
+            rows.at[k, pl.ds(0, 2)], rows.at[k, pl.ds(2, 2)], cs.at[k], cr.at[k], me, core
+        )
+        for k in range(steps)
+    ]
+    c_out = [
+        remote(part.at[k, pl.ds(2, 2)], from_core.at[k], ps.at[k], pr.at[k], me, core)
+        for k in range(steps)
+    ]
+    x_out = [
+        remote(to_x.at[k], from_x.at[k], qs.at[k], qr.at[k], me, across) for k in range(steps)
+    ]
+    z_out = [None] + [
+        remote(total.at[k], back_ref.at[me], bs.at[k], br.at[k], peers[k], lane)
+        for k in range(1, steps)
+    ]
+
+    def stage_a(k):
+        if k > 0:
+            z_in[k].wait_recv()
+        x_in[k].start()
+
+    def stage_b(k):
+        x_in[k].wait_recv()
+        c_in[k].start()
+
+    def stage_c(k):
+        c_in[k].wait_recv()
+
+        @pl.loop(0, hidden // tile)
+        def _(i):
+            cols = pl.ds(pl.multiple_of(i * tile, tile), tile)
+            block = rows[k].reshape(4 * cap, width)
+            gate = jnp.dot(block, gate_ref[:, cols], preferred_element_type=jnp.float32)
+            up = jnp.dot(block, up_ref[:, cols], preferred_element_type=jnp.float32)
+            act[:, cols] = (gate / (1.0 + jnp.exp(-gate)) * up).astype(jnp.bfloat16)
+
+        @pl.loop(0, width // tile_out)
+        def _(i):
+            cols = pl.ds(pl.multiple_of(i * tile_out, tile_out), tile_out)
+            summed = jnp.dot(act[...], down_ref[:, cols], preferred_element_type=jnp.float32)
+            part[k, :, :, cols] = summed.astype(jnp.bfloat16).reshape(4, cap, tile_out)
+
+        c_out[k].start()
+
+    def stage_d(k):
+        c_out[k].wait_recv()
+        to_x[k] = (
+            part[k, 1].astype(jnp.float32) + from_core[k, 1].astype(jnp.float32)
+        ).astype(jnp.bfloat16)
+        x_out[k].start()
+
+    def stage_e(k):
+        x_out[k].wait_recv()
+        summed = (
+            part[k, 0].astype(jnp.float32)
+            + from_core[k, 0].astype(jnp.float32)
+            + from_x[k].astype(jnp.float32)
+        ).astype(jnp.bfloat16)
+        if k == 0:
+            back_ref[me] = summed
+        else:
+            total[k] = summed
+            z_out[k].start()
+
+    for k in range(1, steps):
+        z_in[k].start()
+    rows[0, 0] = out_ref[me]
+    stage_a(0)
+    stage_b(0)
+    for k in range(steps):
+        if k > 0:
+            stage_d(k - 1)
+        if k + 1 < steps:
+            stage_a(k + 1)
+        stage_c(k)
+        if k > 0:
+            stage_e(k - 1)
+        if k + 1 < steps:
+            stage_b(k + 1)
+    stage_d(steps - 1)
+    stage_e(steps - 1)
+    for k in range(steps):
+        if k > 0:
+            z_out[k].wait_recv()
+            z_in[k].wait_send()
+            z_out[k].wait_send()
+        for copy in (x_in[k], c_in[k], c_out[k], x_out[k]):
+            copy.wait_send()
+
+
+def exchange(outgoing, gate, up, down):
+    steps, cap, width = outgoing.shape
+    hidden = gate.shape[1]
+    vmem = pl.BlockSpec(memory_space=pltpu.VMEM)
+    kind = jnp.bfloat16
+    return pl.pallas_call(
+        functools.partial(exchange_kernel, steps),
+        out_shape=jax.ShapeDtypeStruct((steps, cap, width), kind),
+        in_specs=[vmem] * 4,
+        out_specs=vmem,
+        scratch_shapes=[
+            pltpu.VMEM((steps, 4, cap, width), kind),
+            pltpu.VMEM((4 * cap, hidden), kind),
+            pltpu.VMEM((steps, 4, cap, width), kind),
+            pltpu.VMEM((steps, 2, cap, width), kind),
+            pltpu.VMEM((steps, cap, width), kind),
+            pltpu.VMEM((steps, cap, width), kind),
+            pltpu.VMEM((steps, cap, width), kind),
+        ]
+        + [pltpu.SemaphoreType.DMA((steps,))] * 12,
+        compiler_params=pltpu.CompilerParams(
+            collective_id=0, has_side_effects=True, vmem_limit_bytes=60 * 1024 * 1024
+        ),
+    )(outgoing, gate, up, down)
+
+
+def fits_exchange(lanes, steps, local_experts, cap, width, hidden):
+    blocks = 14 * steps * cap * width * 2 + 3 * width * hidden * 2
+    return (
+        lanes == 4
+        and local_experts == 1
+        and steps & (steps - 1) == 0
+        and steps <= 8
+        and cap % 16 == 0
+        and blocks < 44 * 1024 * 1024
+    )
+
+
+def exchange_plain(outgoing, gate_proj, up_proj, down_proj):
+    rows_in = lax.all_gather(
+        lax.all_to_all(outgoing, "ep", split_axis=0, concat_axis=0, tiled=True),
+        "tp",
+        axis=0,
+        tiled=True,
+    )
+    gate_out = jnp.einsum("secd,edf->secf", rows_in, gate_proj, preferred_element_type=jnp.float32)
+    up_out = jnp.einsum("secd,edf->secf", rows_in, up_proj, preferred_element_type=jnp.float32)
+    active = (jax.nn.silu(gate_out) * up_out).astype(jnp.bfloat16)
+    summed = lax.psum_scatter(
+        jnp.einsum("secf,efd->secd", active, down_proj, preferred_element_type=jnp.float32).astype(
+            jnp.bfloat16
+        ),
+        "tp",
+        scatter_dimension=0,
+        tiled=True,
+    )
+    return lax.all_to_all(summed, "ep", split_axis=0, concat_axis=0, tiled=True)
 
 
 def both_halves(
@@ -145,28 +377,29 @@
         jnp.bfloat16
     )
     outgoing = outgoing.reshape(expert_axis, local_experts, capacity, model_dim)
-    arrived = lax.all_to_all(outgoing, "ep", split_axis=0, concat_axis=0, tiled=True)
-    arrived, query_rows, projected_keys, projected_values = lax.optimization_barrier(
-        (arrived, query_rows, projected_keys, projected_values)
-    )
-    rows_in = lax.all_gather(arrived, "tp", axis=0, tiled=True)
     head_partial = mixer_half(
         query_rows, projected_keys, projected_values, query_gain, key_norm_gain, out_proj
     )
-    rows_in, head_partial = lax.optimization_barrier((rows_in, head_partial))
-    mixed_rows = lax.psum_scatter(head_partial, "tp", scatter_dimension=0, tiled=True)
-    gate_out = jnp.einsum("secd,edf->secf", rows_in, gate_proj, preferred_element_type=jnp.float32)
-    up_out = jnp.einsum("secd,edf->secf", rows_in, up_proj, preferred_element_type=jnp.float32)
-    active = (jax.nn.silu(gate_out) * up_out).astype(jnp.bfloat16)
-    summed = lax.psum_scatter(
-        jnp.einsum("secf,efd->secd", active, down_proj, preferred_element_type=jnp.float32).astype(
-            jnp.bfloat16
-        ),
+    lanes = lax.axis_size("tp")
+    pieces = lax.all_to_all(
+        head_partial.reshape(lanes, -1, head_partial.shape[1]),
         "tp",
-        scatter_dimension=0,
+        split_axis=0,
+        concat_axis=0,
         tiled=True,
     )
-    returned = lax.all_to_all(summed, "ep", split_axis=0, concat_axis=0, tiled=True)
+    mixed_rows = jnp.sum(pieces.astype(jnp.float32), axis=0).astype(jnp.bfloat16)
+    if fits_exchange(
+        lanes, expert_axis, local_experts, capacity, model_dim, gate_proj.shape[2]
+    ):
+        returned = exchange(
+            outgoing.reshape(expert_axis, capacity, model_dim),
+            gate_proj.reshape(gate_proj.shape[1:]),
+            up_proj.reshape(up_proj.shape[1:]),
+            down_proj.reshape(down_proj.shape[1:]),
+        )
+    else:
+        returned = exchange_plain(outgoing, gate_proj, up_proj, down_proj)
     results = returned.reshape(experts_all * capacity, model_dim)
     first_weight = jax.nn.sigmoid(expert_score[:, 0] - expert_score[:, 1])
     picks = target.reshape(length, top_count)

time: 236 us -> 150 us (0.64)
  the two profiles are of different devices: /device:TPU:0 before, /device:TPU:16 now
where the time goes in v2:
time: 150 us; the launch traced here: 149 us
  Pallas kernels  109 us (73%)
  matrix products  14 us (9%)
  blocking collectives  12.8 us (9%)
  other arithmetic  5 us (3%)
  local copies, waits for them, and re-layouts  4.26 us (3%)
  starting transfers between devices  3.62 us (2%)
    pallas_call x1, Pallas kernels, exchange(): pl.pallas_call(functools.partial(exchange_kernel, steps), out_shape=jax.S...  109 us
    all_gather x1, blocking collectives, mixer_half(): lax.all_gather(jnp.concatenate([keys_turned, projected_values], axis=1),...  12.8 us
    dot_general x3, matrix products, one_block(): jnp.einsum('tkgd,skd->kgts', query_matrix, key_block, preferred_element_t...  3.75 us
    dot_general x3, matrix products, one_block(): jnp.einsum('kgts,skd->tkgd', weights.astype(jnp.bfloat16), value_block, p...  3.66 us
    all_to_all x1, starting transfers between devices, both_halves(): lax.all_to_all(head_partial.reshape(lanes, -1, head_partial.shape[1]), 't...  3.62 us
    dot_general x2, matrix products, both_halves(): jnp.dot((picks[:, k:k + 1] == jnp.arange(experts_all * capacity, dtype=jn...  3.3 us
  transfers between devices with their start and end apart: 1, of which 0 were waited for; matrix products, arithmetic and copies ran while one was open for 5% of the time, Pallas kernels for 73%

profile of v2, /device:TPU:16, one launch (start us, length us, event | category | flops | bytes accessed | tf_op | source)
XLA Modules:
  0.0 149.4 jit_solution(15455439856798924071)
XLA Ops:
  0.7 1.2 copy.76
  2.0 0.7 mul.309
  2.9 0.2 fusion.31
  3.9 0.3 subtract_convert_fusion.1
  4.3 12.8 %all_gather.3 = bf16[768,256]{1,0:T(8,128)(2,1)S(1)} all-gather(bf16[192,256]{1,0:T(8,128)(2,1)S(1)} %copy.75), channel_id=1, replica_groups=mesh['grp'=2,'ep'=4,'tp'=4] {'ep'}, dimensions={0}, use_global_device_ids=true | all-gather | bytes 491520 | tf_op jit(solution)/shard_map/all_gather | solution.py:66
  17.1 0.8 fusion.43
  17.9 8.8 %while.18 = (s32[]{:T(128)}, f32[1,4,192]{2,1,0:T(4,128)S(1)}, f32[1,4,192]{2,1,0:T(4,128)S(1)}, f32[192,1,4,128]{3,0,2,1:T(8,128)S(1)}, bf16[768,128]{1,0:T(8,1...) while((s32[]{:T(128)}, f32[1,4,192]{2,1,0:T(4,128)S(1)}, ...), condition=%wide.region_5.6_spmd.clone, body=%wide.region_2.0_spmd.clone.sunk | while | flops 102142472 | bytes 3522735 | solution.py:102
  17.9 1.2 fusion.55
  19.2 1.2 fusion.58
  20.4 0.4 fusion.57
  20.8 1.3 fusion.55
  22.1 1.2 fusion.58
  23.3 0.4 fusion.57
  23.7 1.3 fusion.55
  25.0 1.2 fusion.58
  26.2 0.4 fusion.57
  27.0 1.5 convolution_convert_fusion.1
  28.5 3.6 %all-to-all-start = ((bf16[4,48,2048]{2,1,0:T(8,128)(2,1)}), bf16[4,48,2048]{2,1,0:T(8,128)(2,1)S(1)}, u32[]{:S(2)}, u32[]{:S(2)}) async-start(bf16[4,48,2048]{2,1,0:T(8,128)(2,1)} %bitcast.110), calls=%async_computation | async-start | bytes 1572864 | tf_op jit(solution)/shard_map/all_to_all | solution.py:384
  32.5 1.2 reduce-window.6
  34.8 1.8 %convolution_convert_fusion = bf16[384,2048]{1,0:T(8,128)(2,1)} fusion(bf16[128,2048]{1,0:T(8,128)(2,1)S(1)} %copy-done.2, f32[2048]{0:T(1024)S(1)} %copy-done.5, f32[128]{0:T(128)S(1)} %add_rsqrt_fusion.2, s32[128,384]{1,0:T(8,128)S(1)} %convert_reduce_fusion), kind=kOutput, calls=%fused_computation.22 | convolution fusion | flops 203210752 | bytes 2302464 | tf_op jit(solution)/shard_map/re,rd->ed/dot_general | solution.py:376
  36.6 108.6 %shard_map.140 = bf16[4,96,2048]{2,1,0:T(8,128)(2,1)} custom-call(bf16[4,96,2048]{2,1,0:T(8,128)(2,1)} %bitcast.109, bf16[2048,512]{1,0:T(8,128)(2,1)} %bitcast.114, bf16[2048,512]{1,0:T(8,128)(2,1)} %bitcast.115, bf16[512,2048]{1,0:T(8,128)(2,1)} %bitcast.116), custom_call_target="tpu_custom_call" | custom-call | tf_op jit(solution)/shard_map/pallas_call | solution.py:285
  145.2 2.0 %convolution_multiply_fusion.2 = f32[128,2048]{1,0:T(8,128)S(1)} fusion(bf16[384,2048]{1,0:T(8,128)(2,1)} %bitcast.107, f32[128]{0:T(128)S(1)} %bitcast.123, s32[128]{0:T(128)S(1)} %get-tuple-element.221), kind=kOutput, calls=%fused_computation.26 | convolution fusion | flops 201637888 | bytes 2622464 | tf_op jit(solution)/shard_map/dot_general | solution.py:407
  147.2 1.3 fusion.16
  148.5 0.8 reduce_sum.74
  (69 shorter events, 2.9 us)
Async XLA Ops:
  0.6 26.4 %copy-start = (bf16[512,2048]{1,0:T(8,128)(2,1)S(1)}, bf16[512,2048]{1,0:T(8,128)(2,1)}, u32[]{:S(2)}) copy-start(bf16[512,2048]{1,0:T(8,128)(2,1)} %param.20) | copy-start | bytes 6291460
  2.0 1.5 %copy-start.3 = (bf16[192,128]{1,0:T(8,128)(2,1)S(1)}, bf16[192,128]{1,0:T(8,128)(2,1)}, u32[]{:S(2)}) copy-start(bf16[192,128]{1,0:T(8,128)(2,1)} %param.16) | copy-start | bytes 147460
  2.8 0.9 copy-start.4
  2.9 1.0 copy-start.8
  27.0 5.1 %copy-start.6 = (s32[128,2]{0,1:T(2,128)S(1)}, s32[128,2]{0,1:T(2,128)}, u32[]{:S(2)}) copy-start(s32[128,2]{0,1:T(2,128)} %param.23) | copy-start | bytes 3076
  28.5 6.1 %copy-start.2 = (bf16[128,2048]{1,0:T(8,128)(2,1)S(1)}, bf16[128,2048]{1,0:T(8,128)(2,1)}, u32[]{:S(2)}) copy-start(bf16[128,2048]{1,0:T(8,128)(2,1)} %param.21) | copy-start | bytes 1572868
  28.5 6.3 %copy-start.7 = (f32[128,2]{0,1:T(2,128)S(1)}, f32[128,2]{0,1:T(2,128)}, u32[]{:S(2)}) copy-start(f32[128,2]{0,1:T(2,128)} %param.24) | copy-start | bytes 3076
  28.5 6.3 %copy-start.5 = (f32[2048]{0:T(1024)S(1)}, f32[2048]{0:T(1024)}, u32[]{:S(2)}) copy-start(f32[2048]{0:T(1024)} %param.22) | copy-start | bytes 24580
  28.5 120.0 %all-to-all-start = ((bf16[4,48,2048]{2,1,0:T(8,128)(2,1)}), bf16[4,48,2048]{2,1,0:T(8,128)(2,1)S(1)}, u32[]{:S(2)}, u32[]{:S(2)}) async-start(bf16[4,48,2048]{2,1,0:T(8,128)(2,1)} %bitcast.110), calls=%async_computation | async-start | bytes 1572864 | tf_op jit(solution)/shard_map/all_to_all | solution.py:384
  145.2 2.0 %copy-start.1 = (bf16[4,96,2048]{2,1,0:T(8,128)(2,1)S(1)}, bf16[4,96,2048]{2,1,0:T(8,128)(2,1)}, u32[]{:S(2)}) copy-start(bf16[4,96,2048]{2,1,0:T(8,128)(2,1)} %shard_map.140) | copy-start | bytes 4718596

commit v3 on v2

--- a/solution.py
+++ b/solution.py
@@ -43,19 +43,27 @@
     return rotate_grid(head_norm(vectors, gain), token_positions).astype(jnp.bfloat16)
 
 
-def mixer_half(query_rows, projected_keys, projected_values, query_gain, key_norm_gain, out_proj):
+def mixer_prepare(query_rows, projected_keys, projected_values, query_gain, key_norm_gain):
     length = query_rows.shape[0]
     head_dim = query_gain.shape[0]
     kv_heads = projected_keys.shape[1] // head_dim
     q_heads = query_rows.shape[1] // head_dim
-    queries_per_group = q_heads // kv_heads
     token_positions = lax.axis_index("ep") * length + jnp.arange(length, dtype=jnp.int32)
     query_matrix = prepare_inputs(query_rows, query_gain, q_heads, token_positions).reshape(
-        length, kv_heads, queries_per_group, head_dim
+        length, q_heads * head_dim
     )
     keys_turned = prepare_inputs(projected_keys, key_norm_gain, kv_heads, token_positions).reshape(
         length, kv_heads * head_dim
     )
+    return query_matrix, jnp.concatenate([keys_turned, projected_values], axis=1)
+
+
+def attend_plain(query_matrix, own_pair, head_dim):
+    length = query_matrix.shape[0]
+    kv_heads = own_pair.shape[1] // (2 * head_dim)
+    q_heads = query_matrix.shape[1] // head_dim
+    queries_per_group = q_heads // kv_heads
+    query_matrix = query_matrix.reshape(length, kv_heads, queries_per_group, head_dim)
     score_scale = head_dim ** (-0.5)
     initial = (
         jnp.full((kv_heads, queries_per_group, length), -1e30, jnp.float32),
@@ -63,9 +71,7 @@
         jnp.zeros((length, kv_heads, queries_per_group, head_dim), jnp.float32),
     )
     width = kv_heads * head_dim
-    pair = lax.all_gather(
-        jnp.concatenate([keys_turned, projected_values], axis=1), "ep", axis=0, tiled=True
-    )
+    pair = lax.all_gather(own_pair, "ep", axis=0, tiled=True)
     key_piece = pair[:, :width]
     value_piece = pair[:, width:]
     piece_rows = key_piece.shape[0]
@@ -100,12 +106,11 @@
         return (new_max, run_sum, run_acc)
 
     run_max, run_sum, run_acc = lax.fori_loop(0, piece_rows // step_rows, one_block, initial)
-    heads_out = (
+    return (
         (run_acc / jnp.transpose(run_sum, (2, 0, 1))[..., None])
         .astype(jnp.bfloat16)
         .reshape(length, q_heads * head_dim)
     )
-    return jnp.dot(heads_out, out_proj, preferred_element_type=jnp.float32).astype(jnp.bfloat16)
 
 
 def flip(index, bits):
@@ -123,7 +128,10 @@
     gate_ref,
     up_ref,
     down_ref,
+    query_ref,
+    pair_ref,
     back_ref,
+    heads_ref,
     rows,
     act,
     part,
@@ -131,6 +139,7 @@
     to_x,
     from_x,
     total,
+    pairs,
     zs,
     zr,
     xs,
@@ -143,6 +152,8 @@
     qr,
     bs,
     br,
+    ks,
+    kr,
 ):
     me = lax.axis_index("ep")
     lane = lax.axis_index("tp")
@@ -172,6 +183,10 @@
 
     z_in = [None] + [
         remote(out_ref.at[peers[k]], rows.at[k, 0], zs.at[k], zr.at[k], peers[k], lane)
+        for k in range(1, steps)
+    ]
+    kv_in = [None] + [
+        remote(pair_ref, pairs.at[k], ks.at[k], kr.at[k], peers[k], lane)
         for k in range(1, steps)
     ]
     x_in = [
@@ -251,14 +266,43 @@
             total[k] = summed
             z_out[k].start()
 
+    def attend():
+        for k in range(1, steps):
+            kv_in[k].wait_recv()
+        held = steps * pair_ref.shape[0]
+        dim = pair_ref.shape[1] // 2
+        keys = pairs[:, :, :dim].reshape(held, dim)
+        values = pairs[:, :, dim:].reshape(held, dim)
+        for head in range(query_ref.shape[1] // dim):
+            cols = slice(head * dim, (head + 1) * dim)
+            scores = (
+                lax.dot_general(
+                    query_ref[:, cols],
+                    keys,
+                    (((1,), (1,)), ((), ())),
+                    preferred_element_type=jnp.float32,
+                )
+                * dim ** (-0.5)
+            )
+            probs = jnp.exp(scores - jnp.max(scores, axis=-1, keepdims=True))
+            amount = jnp.sum(probs, axis=-1, keepdims=True)
+            summed = jnp.dot(
+                probs.astype(jnp.bfloat16), values, preferred_element_type=jnp.float32
+            )
+            heads_ref[:, cols] = (summed / amount).astype(jnp.bfloat16)
+
     for k in range(1, steps):
+        kv_in[k].start()
         z_in[k].start()
     rows[0, 0] = out_ref[me]
+    pairs[0] = pair_ref[...]
     stage_a(0)
     stage_b(0)
     for k in range(steps):
         if k > 0:
             stage_d(k - 1)
+        if k == 1:
+            attend()
         if k + 1 < steps:
             stage_a(k + 1)
         stage_c(k)
@@ -272,21 +316,25 @@
         if k > 0:
             z_out[k].wait_recv()
             z_in[k].wait_send()
+            kv_in[k].wait_send()
             z_out[k].wait_send()
         for copy in (x_in[k], c_in[k], c_out[k], x_out[k]):
             copy.wait_send()
 
 
-def exchange(outgoing, gate, up, down):
+def exchange(outgoing, gate, up, down, queries, pair):
     steps, cap, width = outgoing.shape
     hidden = gate.shape[1]
     vmem = pl.BlockSpec(memory_space=pltpu.VMEM)
     kind = jnp.bfloat16
     return pl.pallas_call(
         functools.partial(exchange_kernel, steps),
-        out_shape=jax.ShapeDtypeStruct((steps, cap, width), kind),
-        in_specs=[vmem] * 4,
-        out_specs=vmem,
+        out_shape=(
+            jax.ShapeDtypeStruct((steps, cap, width), kind),
+            jax.ShapeDtypeStruct(queries.shape, kind),
+        ),
+        in_specs=[vmem] * 6,
+        out_specs=(vmem, vmem),
         scratch_shapes=[
             pltpu.VMEM((steps, 4, cap, width), kind),
             pltpu.VMEM((4 * cap, hidden), kind),
@@ -295,21 +343,25 @@
             pltpu.VMEM((steps, cap, width), kind),
             pltpu.VMEM((steps, cap, width), kind),
             pltpu.VMEM((steps, cap, width), kind),
+            pltpu.VMEM((steps,) + pair.shape, kind),
         ]
-        + [pltpu.SemaphoreType.DMA((steps,))] * 12,
+        + [pltpu.SemaphoreType.DMA((steps,))] * 14,
         compiler_params=pltpu.CompilerParams(
             collective_id=0, has_side_effects=True, vmem_limit_bytes=60 * 1024 * 1024
         ),
-    )(outgoing, gate, up, down)
-
-
-def fits_exchange(lanes, steps, local_experts, cap, width, hidden):
+    )(outgoing, gate, up, down, queries, pair)
+
+
+def fits_exchange(lanes, steps, local_experts, cap, width, hidden, length, kv_heads):
     blocks = 14 * steps * cap * width * 2 + 3 * width * hidden * 2
     return (
         lanes == 4
         and local_experts == 1
         and steps & (steps - 1) == 0
-        and steps <= 8
+        and 1 < steps <= 8
+        and kv_heads == 1
+        and length % 16 == 0
+        and length <= 256
         and cap % 16 == 0
         and blocks < 44 * 1024 * 1024
     )
@@ -377,10 +429,35 @@
         jnp.bfloat16
     )
     outgoing = outgoing.reshape(expert_axis, local_experts, capacity, model_dim)
-    head_partial = mixer_half(
-        query_rows, projected_keys, projected_values, query_gain, key_norm_gain, out_proj
-    )
     lanes = lax.axis_size("tp")
+    head_dim = query_gain.shape[0]
+    queries, pair = mixer_prepare(
+        query_rows, projected_keys, projected_values, query_gain, key_norm_gain
+    )
+    if fits_exchange(
+        lanes,
+        expert_axis,
+        local_experts,
+        capacity,
+        model_dim,
+        gate_proj.shape[2],
+        queries.shape[0],
+        pair.shape[1] // (2 * head_dim),
+    ):
+        returned, heads_out = exchange(
+            outgoing.reshape(expert_axis, capacity, model_dim),
+            gate_proj.reshape(gate_proj.shape[1:]),
+            up_proj.reshape(up_proj.shape[1:]),
+            down_proj.reshape(down_proj.shape[1:]),
+            queries,
+            pair,
+        )
+    else:
+        heads_out = attend_plain(queries, pair, head_dim)
+        returned = exchange_plain(outgoing, gate_proj, up_proj, down_proj)
+    head_partial = jnp.dot(heads_out, out_proj, preferred_element_type=jnp.float32).astype(
+        jnp.bfloat16
+    )
     pieces = lax.all_to_all(
         head_partial.reshape(lanes, -1, head_partial.shape[1]),
         "tp",
@@ -389,17 +466,6 @@
         tiled=True,
     )
     mixed_rows = jnp.sum(pieces.astype(jnp.float32), axis=0).astype(jnp.bfloat16)
-    if fits_exchange(
-        lanes, expert_axis, local_experts, capacity, model_dim, gate_proj.shape[2]
-    ):
-        returned = exchange(
-            outgoing.reshape(expert_axis, capacity, model_dim),
-            gate_proj.reshape(gate_proj.shape[1:]),
-            up_proj.reshape(up_proj.shape[1:]),
-            down_proj.reshape(down_proj.shape[1:]),
-        )
-    else:
-        returned = exchange_plain(outgoing, gate_proj, up_proj, down_proj)
     results = returned.reshape(experts_all * capacity, model_dim)
     first_weight = jax.nn.sigmoid(expert_score[:, 0] - expert_score[:, 1])
     picks = target.reshape(length, top_count)

time: 150 us -> 144 us (0.960)
  the two profiles are of different devices: /device:TPU:16 before, /device:TPU:8 now
where the time goes in v3:
time: 144 us; the launch traced here: 143 us
  Pallas kernels  115 us (80%)
  waiting for transfers between devices  8.23 us (6%)
  matrix products  7.51 us (5%)
  local copies, waits for them, and re-layouts  4.56 us (3%)
  other arithmetic  4.23 us (3%)
  starting transfers between devices  3.49 us (2%)
    pallas_call x1, Pallas kernels, exchange(): pl.pallas_call(functools.partial(exchange_kernel, steps), out_shape=(jax....  115 us
    all_to_all x1, waiting for transfers between devices, both_halves(): lax.all_to_all(head_partial.reshape(lanes, -1, head_partial.shape[1]), 't...  8.23 us
    all_to_all x1, starting transfers between devices, both_halves(): lax.all_to_all(head_partial.reshape(lanes, -1, head_partial.shape[1]), 't...  3.49 us
    dot_general x2, matrix products, both_halves(): jnp.dot((picks[:, k:k + 1] == jnp.arange(experts_all * capacity, dtype=jn...  3.3 us
  transfers between devices with their start and end apart: 1, of which 1 were waited for; matrix products, arithmetic and copies ran while one was open for 2% of the time, Pallas kernels for 0%

profile of v3, /device:TPU:8, one launch (start us, length us, event | category | flops | bytes accessed | tf_op | source)
XLA Modules:
  0.0 143.4 jit_solution(9708661730634202304)
XLA Ops:
  0.7 0.9 copy.52
  1.6 0.1 eq.76
  1.7 0.1 eq.72
  1.9 1.1 copy.57
  3.1 0.7 mul.253
  3.9 0.2 fusion.16
  4.2 0.1 multiply_multiply_fusion
  4.5 0.8 copy.60.query_ref
  5.3 0.1 copy.58
  5.5 0.3 subtract_convert_fusion.1
  5.8 0.1 copy.59
  5.9 1.2 reduce-window.6
  7.6 0.1 reduce_sum.60
  7.8 0.1 convert_reduce_fusion
  7.9 0.2 fusion.2
  8.1 0.7 pad_maximum_fusion.1.pair_ref
  8.8 1.8 %convolution_convert_fusion = bf16[384,2048]{1,0:T(8,128)(2,1)} fusion(bf16[128,2048]{1,0:T(8,128)(2,1)S(1)} %copy-done.2, f32[2048]{0:T(1024)S(1)} %copy-done.5, f32[128]{0:T(128)S(1)} %add_rsqrt_fusion.2, s32[128,384]{1,0:T(8,128)S(1)} %convert_reduce_fusion), kind=kOutput, calls=%fused_computation | convolution fusion | flops 203210752 | bytes 2302464 | tf_op jit(solution)/shard_map/re,rd->ed/dot_general | solution.py:428
  10.6 114.5 %shard_map.140 = (bf16[4,96,2048]{2,1,0:T(8,128)(2,1)}, bf16[192,512]{1,0:T(8,128)(2,1)}) custom-call(bf16[4,96,2048]{2,1,0:T(8,128)(2,1)} %bitcast.49, bf16[2048,512]{1,0:T(8,128)(2,1)} %bitcast.52, bf16[2048,512]{1,0:T(8,128)(2,1)} %bitcast.53, bf16[512,2048]{1,0:T(8,128)(2,1)} %bitcast.54, bf16[192,512]{1,0:T(8,128)(2,1)} %copy.60.query_ref, ...), custom_call_target="tpu_custom_call" | custom-call | tf_op jit(solution)/shard_map/pallas_call | solution.py:330
  125.1 2.4 %convolution_convert_fusion.1 = bf16[192,2048]{1,0:T(8,128)(2,1)} fusion(bf16[192,512]{1,0:T(8,128)(2,1)} %get-tuple-element.4, bf16[512,2048]{1,0:T(8,128)(2,1)S(1)} %copy-done), kind=kOutput, calls=%fused_computation.1 | convolution fusion | flops 403046400 | bytes 3080192 | tf_op jit(solution)/shard_map/dot_general | solution.py:458
  127.5 3.5 %all-to-all-start = ((bf16[4,48,2048]{2,1,0:T(8,128)(2,1)}), bf16[4,48,2048]{2,1,0:T(8,128)(2,1)S(1)}, u32[]{:S(2)}, u32[]{:S(2)}) async-start(bf16[4,48,2048]{2,1,0:T(8,128)(2,1)} %bitcast.50), calls=%async_computation | async-start | bytes 1572864 | tf_op jit(solution)/shard_map/all_to_all | solution.py:461
  131.1 2.0 %convolution_multiply_fusion.1 = f32[128,2048]{1,0:T(8,128)S(1)} fusion(bf16[384,2048]{1,0:T(8,128)(2,1)} %bitcast.47, f32[128]{0:T(128)S(1)} %bitcast.59, s32[128]{0:T(128)S(1)} %get-tuple-element.19), kind=kOutput, calls=%fused_computation.4 | convolution fusion | flops 201637888 | bytes 2622464 | tf_op jit(solution)/shard_map/dot_general | solution.py:473
  133.1 1.3 fusion.1
  134.4 8.2 %all-to-all-done = bf16[4,48,2048]{2,1,0:T(8,128)(2,1)S(1)} async-done(((bf16[4,48,2048]{2,1,0:T(8,128)(2,1)}), bf16[4,48,2048]{2,1,0:T(8,128)(2,1)S(1)}, u32[]{:S(2)}, u32[]{:S(2)}) %all-to-all-start) | async-done | bytes 786464 | tf_op jit(solution)/shard_map/all_to_all | solution.py:461
  142.6 0.8 reduce_sum.65
  (42 shorter events, 1.0 us)
Async XLA Ops:
  0.6 124.5 %copy-start = (bf16[512,2048]{1,0:T(8,128)(2,1)S(1)}, bf16[512,2048]{1,0:T(8,128)(2,1)}, u32[]{:S(2)}) copy-start(bf16[512,2048]{1,0:T(8,128)(2,1)} %param.18) | copy-start | bytes 6291460
  3.0 2.2 %copy-start.3 = (bf16[192,128]{1,0:T(8,128)(2,1)S(1)}, bf16[192,128]{1,0:T(8,128)(2,1)}, u32[]{:S(2)}) copy-start(bf16[192,128]{1,0:T(8,128)(2,1)} %param.14) | copy-start | bytes 147460
  3.9 1.5 %copy-start.8 = (f32[128]{0:T(128)S(1)}, f32[128]{0:T(128)}, u32[]{:S(2)}) copy-start(f32[128]{0:T(128)} %param.17) | copy-start | bytes 1540
  4.3 3.5 %copy-start.6 = (s32[128,2]{0,1:T(2,128)S(1)}, s32[128,2]{0,1:T(2,128)}, u32[]{:S(2)}) copy-start(s32[128,2]{0,1:T(2,128)} %param.21) | copy-start | bytes 3076
  4.3 3.6 %copy-start.2 = (bf16[128,2048]{1,0:T(8,128)(2,1)S(1)}, bf16[128,2048]{1,0:T(8,128)(2,1)}, u32[]{:S(2)}) copy-start(bf16[128,2048]{1,0:T(8,128)(2,1)} %param.19) | copy-start | bytes 1572868
  4.4 3.7 %copy-start.4 = (bf16[192,128]{1,0:T(8,128)(2,1)S(1)}, bf16[192,128]{1,0:T(8,128)(2,1)}, u32[]{:S(2)}) copy-start(bf16[192,128]{1,0:T(8,128)(2,1)} %param.15) | copy-start | bytes 147460
  4.4 4.4 %copy-start.5 = (f32[2048]{0:T(1024)S(1)}, f32[2048]{0:T(1024)}, u32[]{:S(2)}) copy-start(f32[2048]{0:T(1024)} %param.20) | copy-start | bytes 24580
  125.1 5.9 %copy-start.7 = (f32[128,2]{0,1:T(2,128)S(1)}, f32[128,2]{0,1:T(2,128)}, u32[]{:S(2)}) copy-start(f32[128,2]{0,1:T(2,128)} %param.22) | copy-start | bytes 3076
  127.5 15.1 %all-to-all-start = ((bf16[4,48,2048]{2,1,0:T(8,128)(2,1)}), bf16[4,48,2048]{2,1,0:T(8,128)(2,1)S(1)}, u32[]{:S(2)}, u32[]{:S(2)}) async-start(bf16[4,48,2048]{2,1,0:T(8,128)(2,1)} %bitcast.50), calls=%async_computation | async-start | bytes 1572864 | tf_op jit(solution)/shard_map/all_to_all | solution.py:461
  131.0 2.1 %copy-start.1 = (bf16[4,96,2048]{2,1,0:T(8,128)(2,1)S(1)}, bf16[4,96,2048]{2,1,0:T(8,128)(2,1)}, u32[]{:S(2)}) copy-start(bf16[4,96,2048]{2,1,0:T(8,128)(2,1)} %get-tuple-element.5) | copy-start | bytes 4718596
